TPU v7x, 32 devices: a whole 2x2x4 slice. The times are simulated.
32 devices in a mesh: grp: 2 (over y), kv: 4 (over z), tp: 4 (over x, core).
Axes of the slice: x: 2, y: 2, z: 4, core: 2. Of those that a mesh axis runs over, the one named last changes fastest.
Arguments:
- residual: bfloat16 [32, 4096], P('grp', ('kv', 'tp')), parts along dimension 0, may hold values from -11 to 11
- cache_keys: bfloat16 [32, 4096, 8, 128], P('grp', 'kv', 'tp'), parts along dimension 0, may hold values from -210 to 210
- cache_values: bfloat16 [32, 4096, 8, 128], P('grp', 'kv', 'tp'), parts along dimension 0, may hold values from -6 to 6
- norm_gain: bfloat16 [4096], P('kv'), may hold values from 0.099609375 to 1.8984375
- query_weight: bfloat16 [4096, 2048], P('kv', 'tp'), may hold values from -0.09375 to 0.09375
- key_weight: bfloat16 [4096, 1024], P('kv', 'tp'), may hold values from -0.25 to 0.25
- value_weight: bfloat16 [4096, 1024], P('kv', 'tp'), may hold values from -0.375 to 0.375
- head_lambda: float32 [16], P('tp'), may hold values from 0.3 to 0.8
- head_gain: bfloat16 [128], replicated, may hold values from 0.099609375 to 1.8984375
- out_weight: bfloat16 [2048, 4096], P('tp', 'kv'), may hold values from -0.1875 to 0.1875
- mixer_gain: bfloat16 [4096], P('kv'), may hold values from 0.099609375 to 1.8984375
- up_weight: bfloat16 [4096, 16384], P('kv', 'tp'), may hold values from -0.09375 to 0.09375
- down_weight: bfloat16 [16384, 4096], P('tp', 'kv'), may hold values from -0.0625 to 0.0625
Outputs:
- updated: bfloat16 [32, 4096], P('grp', ('kv', 'tp')), parts along dimension 0
There are 2 independent parts, one for each index of `grp`. A program takes and returns all parts, laid end to end along the dimension named above; an argument that names none is the same for every part. Nothing has to cross between parts.
All inputs are finite; a program needn't handle non-finite values.
Results may differ from a plain program's by a relative error of at most 0.018.
Values may be sent and summed in bfloat16 or wider, within the bound.
A program may use at most 128 MiB of HBM per device.

v0:
```python
import jax
import jax.numpy as jnp
from jax import lax
from jax.sharding import PartitionSpec as P

D = 4096
HEADS = 16
KV_HEADS = 8
HALF = 64
VDIM = 128


EPS = 1e-06


def joined(shard, axis, combine):
    everything = jax.tree.map(lambda part: lax.all_gather(part, axis), shard)
    first = jax.tree.map(lambda part: part[0], everything)

    def step(k, so_far):
        return combine(so_far, jax.tree.map(lambda part: part[k], everything))

    return lax.fori_loop(1, lax.axis_size(axis), step, first)


def combine(first, second):
    top = jnp.maximum(first[0], second[0])
    left = jnp.exp(first[0] - top)
    right = jnp.exp(second[0] - top)
    return (
        top,
        first[1] * left + second[1] * right,
        first[2] * left[..., None] + second[2] * right[..., None],
    )


def body(
    residual,
    cache_keys,
    cache_values,
    norm_gain,
    query_weight,
    key_weight,
    value_weight,
    head_lambda,
    head_gain,
    out_weight,
    mixer_gain,
    up_weight,
    down_weight,
):
    f32 = jnp.float32
    bf16 = jnp.bfloat16
    rows = residual.shape[0]
    kv_local = cache_keys.shape[2]
    group = HEADS // KV_HEADS
    scale = 1.0 / HALF**0.5
    block = lax.all_gather(residual, "tp", axis=1, tiled=True).astype(f32)
    scaled = (block * norm_gain.astype(f32)).astype(bf16)
    q_part = jnp.dot(scaled, query_weight, preferred_element_type=f32)
    k_part = jnp.dot(scaled, key_weight, preferred_element_type=f32)
    v_part = jnp.dot(scaled, value_weight, preferred_element_type=f32)
    sq_part = jnp.sum(block * block, axis=1)
    q_sum, k_sum, v_sum, sq_sum = lax.psum((q_part, k_part, v_part, sq_part), "kv")
    inv_rms = lax.rsqrt(sq_sum / D + EPS)[:, None]
    query = (inv_rms * q_sum).astype(bf16).reshape(rows, kv_local, group, 2, HALF)
    new_key = (inv_rms * k_sum).astype(bf16).reshape(rows, kv_local, 2, HALF)
    new_value = (inv_rms * v_sum).astype(bf16).reshape(rows, kv_local, VDIM)
    positions = cache_keys.shape[1]
    keys = cache_keys.reshape(rows, positions, kv_local, 2, HALF)
    scores = jnp.einsum("bkgch,bpkch->bkgcp", query, keys, preferred_element_type=f32) * scale
    local_top = jnp.max(scores, axis=4)
    expo = jnp.exp(scores - local_top[..., None])
    local_total = jnp.sum(expo, axis=4)
    local_weighted = jnp.einsum(
        "bkgcp,bpkv->bkgcv", expo.astype(bf16), cache_values, preferred_element_type=f32
    )
    cache_top, total, weighted = joined((local_top, local_total, local_weighted), "kv", combine)
    own = jnp.einsum("bkgch,bkch->bkgc", query, new_key, preferred_element_type=f32) * scale
    top = jnp.maximum(cache_top, own)
    old_part = jnp.exp(cache_top - top)
    own_part = jnp.exp(own - top)
    numer = (
        weighted * old_part[..., None]
        + own_part[..., None] * new_value.astype(f32)[:, :, None, None, :]
    )
    attended = numer / (total * old_part + own_part)[..., None]
    lambdas = head_lambda.reshape(kv_local, group)[None, :, :, None]
    diff = attended[:, :, :, 0] - lambdas * attended[:, :, :, 1]
    normed = (
        diff * lax.rsqrt(jnp.mean(diff * diff, axis=3, keepdims=True) + EPS) * head_gain.astype(f32)
    )
    heads_out = normed.astype(bf16).reshape(rows, kv_local * group * VDIM)
    projected = jnp.dot(heads_out, out_weight, preferred_element_type=f32)
    mixed = (
        residual.astype(f32) + lax.psum_scatter(projected, "tp", scatter_dimension=1, tiled=True)
    ).astype(bf16)
    mixed_block = lax.all_gather(mixed, "tp", axis=1, tiled=True).astype(f32)
    scaled2 = (mixed_block * mixer_gain.astype(f32)).astype(bf16)
    up_part = jnp.dot(scaled2, up_weight, preferred_element_type=f32)
    sq_mixed = jnp.sum(mixed_block * mixed_block, axis=1)
    up_share = lax.psum_scatter(up_part, "kv", scatter_dimension=1, tiled=True)
    sq_total = lax.psum(sq_mixed, "kv")
    inv_rms2 = lax.rsqrt(sq_total / D + EPS)[:, None]
    share = jnp.square(jnp.maximum(inv_rms2 * up_share, 0.0)).astype(bf16)
    hidden = lax.all_gather(share, "kv", axis=1, tiled=True)
    down_part = jnp.dot(hidden, down_weight, preferred_element_type=f32)
    return (
        mixed.astype(f32) + lax.psum_scatter(down_part, "tp", scatter_dimension=1, tiled=True)
    ).astype(bf16)


def solution(mesh):
    in_specs = (
        P("grp", ("kv", "tp")),
        P("grp", "kv", "tp", None),
        P("grp", "kv", "tp", None),
        P("kv"),
        P("kv", "tp"),
        P("kv", "tp"),
        P("kv", "tp"),
        P("tp"),
        P(),
        P("tp", "kv"),
        P("kv"),
        P("kv", "tp"),
        P("tp", "kv"),
    )
    out_specs = P("grp", ("kv", "tp"))
    return jax.shard_map(body, mesh=mesh, in_specs=in_specs, out_specs=out_specs, check_vma=False)
```

profile of v0, /device:TPU:0, one launch (start us, length us, event | category | flops | bytes accessed | tf_op | source)
XLA Modules:
  0.0 212.5 jit_solution(997170010051651746)
XLA Ops:
  6.5 0.8 convert_element_type.64
  7.3 6.4 %all_gather.27 = bf16[16,1024]{1,0:T(8,128)(2,1)S(1)} all-gather(bf16[16,256]{1,0:T(8,128)(2,1)} %param.15), channel_id=1, replica_groups=mesh['grp'=2,'kv'=4,'tp'=4] {'tp'}, dimensions={1}, use_global_device_ids=true | all-gather | bytes 40960 | tf_op jit(solution)/shard_map/all_gather | solution.py:58
  13.8 0.7 fusion.10
  14.4 1.8 fusion.19
  16.2 1.8 fusion.17
  18.1 2.1 fusion.21
  20.2 0.7 mul.232
  21.0 21.2 %copy.77 = bf16[16,1024,2,128]{1,3,2,0:T(8,128)(2,1)} copy(bf16[16,1024,2,128]{3,2,1,0:T(2,128)(2,1)} %param.16) | data formatting | bytes 16777216 | tf_op args[1]
  42.1 14.4 %all-reduce.3.cloned.1.call-done = (f32[16,512]{1,0:T(8,128)}, f32[16]{0:T(128)}, f32[16,256]{1,0:T(8,128)}, f32[16,256]{1,0:T(8,128)}) async-done(((f32[16,512]{1,0:T(8,128)}, f32[16]{0:T(128)}, f32[16,256]{1,0:T(8,128)}, f32[16,256]{1,0:T(8,128)}), (f32[16,512]{1,0:T(8,128)}, f32[16]{0:T(128)}, f32[16,256]{1,0:T(8,128)}, f32[16,256]{1,0:T(8,128)})) %all-reduce.3.cloned.1.call-update) | async-done | bytes 65616 | tf_op jit(solution)/shard_map/psum | solution.py:64
  56.5 0.7 add_rsqrt_fusion.2
  57.2 0.8 multiply_convert_fusion.2
  58.0 0.8 fusion.29
  59.3 4.7 %fusion.35 = (f32[16,2,2,2]{2,3,1,0:T(2,128)S(1)}, f32[16,2,2,2,1024]{4,2,3,1,0:T(2,128)S(1)}) fusion(bf16[16,1024,2,2,64]{1,4,3,2,0:T(8,128)(2,1)} %bitcast.56, bf16[16,2,2,2,64]{4,3,2,1,0:T(2,128)(2,1)S(1)} %reshape.43), kind=kOutput, calls=%fused_computation.55 | convolution fusion | flops 17039232 | bytes 8929792 | tf_op jit(solution)/shard_map/bkgch,bpkch->bkgcp/dot_general | solution.py:71
  64.4 0.5 fusion.7
  64.9 4.8 %fusion.3 = f32[16,2,2,2,128]{4,2,3,1,0:T(2,128)S(1)} fusion(bf16[16,1024,2,128,1]{3,2,1,0,4:T(2,128)(2,1)} %bitcast.65, f32[16,2,2,2,1024]{4,2,3,1,0:T(2,128)S(1)} %get-tuple-element.245, f32[16,2,2,2]{2,3,1,0:T(2,128)S(1)} %get-tuple-element.244), kind=kOutput, calls=%fused_computation.8 | convolution fusion | flops 33816576 | bytes 8978944 | tf_op jit(solution)/shard_map/bkgcp,bpkv->bkgcv/dot_general | solution.py:75
  70.0 13.6 %all-gather.1 = f32[64,2,2,2]{3,2,1,0:T(2,128)S(1)} all-gather(f32[16,2,2,2]{3,2,1,0:T(2,128)S(1)} %copy.80), channel_id=3, replica_groups=mesh['grp'=2,'kv'=4,'tp'=4] {'kv'}, dimensions={0}, use_global_device_ids=true | all-gather | bytes 2560 | tf_op jit(solution)/shard_map/all_gather | solution.py:17
  83.9 13.5 %all-gather = f32[64,2,2,2]{3,2,1,0:T(2,128)S(1)} all-gather(f32[16,2,2,2]{3,2,1,0:T(2,128)S(1)} %copy.79), channel_id=2, replica_groups=mesh['grp'=2,'kv'=4,'tp'=4] {'kv'}, dimensions={0}, use_global_device_ids=true | all-gather | bytes 2560 | tf_op jit(solution)/shard_map/all_gather | solution.py:17
  97.6 13.8 %all-gather.2 = f32[64,2,2,2,128]{4,3,2,1,0:T(2,128)S(1)} all-gather(f32[16,2,2,2,128]{4,3,2,1,0:T(2,128)S(1)} %copy.82), channel_id=4, replica_groups=mesh['grp'=2,'kv'=4,'tp'=4] {'kv'}, dimensions={0}, use_global_device_ids=true | all-gather | bytes 327680 | tf_op jit(solution)/shard_map/all_gather | solution.py:17
  111.4 2.1 while.19
  112.3 0.4 fusion.49
  114.9 0.9 fusion.26
  115.9 19.9 %reduce-scatter.4.cloned.1.call-done = f32[16,256]{1,0:T(8,128)} async-done(((f32[16,1024]{1,0:T(8,128)}), f32[16,256]{1,0:T(8,128)}) %reduce-scatter.4.cloned.1.call-update) | async-done | bytes 16400 | tf_op jit(solution)/shard_map/reduce_scatter | solution.py:96
  135.8 0.7 add_convert_fusion.1
  136.5 5.2 %all_gather.34 = bf16[16,1024]{1,0:T(8,128)(2,1)S(1)} all-gather(bf16[16,256]{1,0:T(8,128)(2,1)S(1)} %add_convert_fusion.1), channel_id=1, replica_groups=mesh['grp'=2,'kv'=4,'tp'=4] {'tp'}, dimensions={1}, use_global_device_ids=true | all-gather | bytes 40960 | tf_op jit(solution)/shard_map/all_gather | solution.py:98
  141.7 5.3 %fusion.14 = f32[16,4096]{1,0:T(8,128)} fusion(bf16[1024,4096]{1,0:T(8,128)(2,1)} %param.26, bf16[16,1024]{1,0:T(8,128)(2,1)S(1)} %all_gather.34, f32[1024]{0:T(1024)S(1)} %convert_element_type.77), kind=kOutput, calls=%fused_computation.26 | convolution fusion | flops 134266880 | bytes 8687616 | tf_op jit(solution)/shard_map/dot_general | solution.py:100
  147.2 11.8 %psum.39 = f32[16]{0:T(128)S(1)} all-reduce(f32[16]{0:T(128)S(1)} %fusion.12), channel_id=1, replica_groups=mesh['grp'=2,'kv'=4,'tp'=4] {'kv'}, use_global_device_ids=true, to_apply=%region_12.0 | all-reduce | flops 16 | bytes 128 | tf_op jit(solution)/shard_map/psum | solution.py:103
  159.0 8.2 %reduce-scatter.6.cloned.1.call-done = f32[16,1024]{1,0:T(8,128)} async-done(((f32[16,4096]{1,0:T(8,128)}), f32[16,1024]{1,0:T(8,128)}) %reduce-scatter.6.cloned.1.call-update) | async-done | bytes 65552 | tf_op jit(solution)/shard_map/reduce_scatter | solution.py:102
  167.2 0.9 multiply_convert_fusion
  168.1 13.4 %all_gather.35 = bf16[16,4096]{1,0:T(8,128)(2,1)S(1)} all-gather(bf16[16,1024]{1,0:T(8,128)(2,1)S(1)} %multiply_convert_fusion), channel_id=1, replica_groups=mesh['grp'=2,'kv'=4,'tp'=4] {'kv'}, dimensions={1}, use_global_device_ids=true | all-gather | bytes 163840 | tf_op jit(solution)/shard_map/all_gather | solution.py:106
  181.5 5.2 %fusion.36 = f32[16,1024]{1,0:T(8,128)} fusion(bf16[16,4096]{1,0:T(8,128)(2,1)S(1)} %all_gather.35, bf16[4096,1024]{1,0:T(8,128)(2,1)} %param.27), kind=kOutput, calls=%fused_computation.56 | convolution fusion | flops 134217728 | bytes 8585216 | tf_op jit(solution)/shard_map/dot_general | solution.py:107
  186.7 18.0 %reduce-scatter.8.cloned.1.call-done = f32[16,256]{1,0:T(8,128)} async-done(((f32[16,1024]{1,0:T(8,128)}), f32[16,256]{1,0:T(8,128)}) %reduce-scatter.8.cloned.1.call-update) | async-done | bytes 16400 | tf_op jit(solution)/shard_map/reduce_scatter | solution.py:109
  204.7 1.3 add_convert_fusion
  (61 shorter events, 5.1 us)
Async XLA Ops:
  6.5 108.4 %copy-start = (bf16[512,1024]{1,0:T(8,128)(2,1)S(1)}, bf16[512,1024]{1,0:T(8,128)(2,1)}, u32[]{:S(2)}) copy-start(bf16[512,1024]{1,0:T(8,128)(2,1)} %param.24) | copy-start | bytes 3145732
  6.5 50.0 %all-reduce.3.cloned.1.call-start = ((), (), s32[]{:S(2)}) async-start(), calls=%async_computation.6 | async-start | bytes 132096 | tf_op jit(solution)/shard_map/psum | solution.py:64
  20.2 115.6 %reduce-scatter.4.cloned.1.call-start = ((), (), s32[]{:S(2)}) async-start(), calls=%async_computation.3 | async-start | bytes 81920 | tf_op jit(solution)/shard_map/reduce_scatter | solution.py:96
  64.0 50.9 %copy-start.3 = (bf16[128]{0:T(256)(128)(2,1)S(1)}, bf16[128]{0:T(256)(128)(2,1)}, u32[]{:S(2)}) copy-start(bf16[128]{0:T(256)(128)(2,1)} %param.23) | copy-start | bytes 772
  64.0 51.8 %copy-start.2 = (bf16[1024]{0:T(1024)(128)(2,1)S(1)}, bf16[1024]{0:T(1024)(128)(2,1)}, u32[]{:S(2)}) copy-start(bf16[1024]{0:T(1024)(128)(2,1)} %param.25) | copy-start | bytes 6148
  64.1 71.8 %copy-start.1 = (bf16[16,256]{1,0:T(8,128)(2,1)S(1)}, bf16[16,256]{1,0:T(8,128)(2,1)}, u32[]{:S(2)}) copy-start(bf16[16,256]{1,0:T(8,128)(2,1)} %param.15) | copy-start | bytes 24580
  115.8 51.3 %reduce-scatter.6.cloned.1.call-start = ((), (), s32[]{:S(2)}) async-start(), calls=%async_computation.4 | async-start | bytes 327680 | tf_op jit(solution)/shard_map/reduce_scatter | solution.py:102
  147.0 57.6 %reduce-scatter.8.cloned.1.call-start = ((), (), s32[]{:S(2)}) async-start(), calls=%async_computation.5 | async-start | bytes 81920 | tf_op jit(solution)/shard_map/reduce_scatter | solution.py:109
Sparse Core Ops, SparseCore 0:
  20.3 36.1 all-reduce.2
  115.9 19.8 reduce-scatter.3
  147.1 19.9 reduce-scatter.5
  186.8 17.8 reduce-scatter.7
where the time goes:
time: 214 us; the launch traced here: 213 us
  blocking collectives  77.6 us (36%)
  waiting for transfers between devices  60.5 us (28%)
  matrix products  26.7 us (12%)
  local copies, waits for them, and re-layouts  25 us (12%)
  between operations  13.3 us (6%)
  other arithmetic  9.24 us (4%)
    all_gather x3, blocking collectives, joined(): everything = jax.tree.map(lambda part: lax.all_gather(part, axis), shard)  40.8 us
    unnamed x9, local copies, waits for them, and re-layouts  21.2 us
    reduce_scatter x1, waiting for transfers between devices, body(): lax.psum_scatter(projected, 'tp', scatter_dimension=1, tiled=True)  19.9 us
    reduce_scatter x1, waiting for transfers between devices, body(): lax.psum_scatter(down_part, 'tp', scatter_dimension=1, tiled=True)  18 us
    psum x1, waiting for transfers between devices, body(): lax.psum((q_part, k_part, v_part, sq_part), 'kv')  14.4 us
    all_gather x1, blocking collectives, body(): hidden = lax.all_gather(share, 'kv', axis=1, tiled=True)  13.4 us
    psum x1, blocking collectives, body(): sq_total = lax.psum(sq_mixed, 'kv')  11.8 us
    reduce_scatter x1, waiting for transfers between devices, body(): up_share = lax.psum_scatter(up_part, 'kv', scatter_dimension=1, tiled=True)  8.16 us
  transfers between devices with their start and end apart: 4, of which 4 were waited for; matrix products, arithmetic and copies ran while one was open for 10% of the time, Pallas kernels for 0%

commit v1 on v0

--- a/solution.py
+++ b/solution.py
@@ -1,6 +1,10 @@
+import functools
+
 import jax
 import jax.numpy as jnp
 from jax import lax
+from jax.experimental import pallas as pl
+from jax.experimental.pallas import tpu as pltpu
 from jax.sharding import PartitionSpec as P
 
 D = 4096
@@ -34,7 +38,7 @@
     )
 
 
-def body(
+def plain_body(
     residual,
     cache_keys,
     cache_values,
@@ -110,7 +114,435 @@
     ).astype(bf16)
 
 
+def spread(column, lanes):
+    high = column.astype(jnp.bfloat16).astype(jnp.float32)
+    lane = lax.broadcasted_iota(jnp.int32, (column.shape[0], lanes), 1)
+    return jnp.where(lane < lanes // 2, high, column - high).astype(jnp.bfloat16)
+
+
+def gathered(pair):
+    pair = pair.astype(jnp.float32)
+    half = pair.shape[1] // 2
+    return pair[:, 0:1] + pair[:, half : half + 1]
+
+
+def layer_kernel(
+    dims,
+    residual_ref,
+    gains_ref,
+    lambda_ref,
+    keys_hbm,
+    values_hbm,
+    qw_hbm,
+    kw_hbm,
+    vw_hbm,
+    ow_hbm,
+    uw_hbm,
+    dw_hbm,
+    out_ref,
+    keys,
+    values,
+    qw,
+    kw,
+    vw,
+    ow,
+    uw,
+    dw,
+    x_all,
+    q_send,
+    q_recv,
+    n_send,
+    n_recv,
+    q_rows,
+    k_rows,
+    v_rows,
+    w_own,
+    w_send,
+    w_recv,
+    s_send,
+    s_recv,
+    att,
+    o_all,
+    o_send,
+    m_send,
+    m_recv,
+    u_send,
+    u_recv,
+    h_send,
+    h_recv,
+    d_send,
+    d_recv,
+    load_sem,
+    cache_sem,
+    x_sem,
+    q_sem,
+    n_sem,
+    w_sem,
+    s_sem,
+    o_sem,
+    m_sem,
+    u_sem,
+    h_sem,
+    d_sem,
+):
+    f32 = jnp.float32
+    bf16 = jnp.bfloat16
+    kvn, tpn, kv_local, groups = dims
+    rows = residual_ref.shape[0]
+    width = residual_ref.shape[1]
+    q_cols = qw.shape[1]
+    k_cols = kw.shape[1]
+    reps = q_cols // VDIM * 2
+    per = rows // groups
+    model = qw.shape[0] * kvn
+    me_kv = lax.axis_index("kv")
+    me_tp = lax.axis_index("tp")
+
+    loads = []
+    for index, (src, dst) in enumerate(((qw_hbm, qw), (kw_hbm, kw), (vw_hbm, vw))):
+        loads.append(pltpu.make_async_copy(src, dst, load_sem.at[index]))
+        loads[-1].start()
+
+    def cache_copy(g, which):
+        src, dst = ((keys_hbm, keys), (values_hbm, values))[which]
+        span = pl.ds(g * per, per)
+        return pltpu.make_async_copy(src.at[span], dst.at[span], cache_sem.at[g, which])
+
+    for g in range(groups):
+        cache_copy(g, 0).start()
+        cache_copy(g, 1).start()
+    for index, (src, dst) in enumerate(((ow_hbm, ow), (uw_hbm, uw), (dw_hbm, dw))):
+        loads.append(pltpu.make_async_copy(src, dst, load_sem.at[3 + index]))
+        loads[-1].start()
+
+    def kv_to(d):
+        return {"kv": lax.rem(me_kv + d, kvn)}
+
+    def tp_to(d):
+        return {"tp": lax.rem(me_tp + d, tpn)}
+
+    def remote(src, dst, sems, index, target):
+        return pltpu.make_async_remote_copy(
+            src_ref=src,
+            dst_ref=dst,
+            send_sem=sems.at[(0,) + index],
+            recv_sem=sems.at[(1,) + index],
+            device_id=target,
+            device_id_type=pl.DeviceIdType.MESH,
+        )
+
+    barrier = pltpu.get_barrier_semaphore()
+    for d in range(1, tpn):
+        pl.semaphore_signal(barrier, 1, device_id=tp_to(d), device_id_type=pl.DeviceIdType.MESH)
+    for d in range(1, kvn):
+        pl.semaphore_signal(barrier, 1, device_id=kv_to(d), device_id_type=pl.DeviceIdType.MESH)
+    pl.semaphore_wait(barrier, tpn + kvn - 2)
+
+    x_copies = [
+        remote(residual_ref, x_all.at[me_tp], x_sem, (d,), tp_to(d)) for d in range(1, tpn)
+    ]
+    for copy in x_copies:
+        copy.start()
+    x_all[me_tp] = residual_ref[...]
+    for copy in x_copies:
+        copy.wait()
+
+    block = jnp.concatenate([x_all[t] for t in range(tpn)], axis=1).astype(f32)
+    scaled = (block * gains_ref[0:1, :]).astype(bf16)
+    sq_own = jnp.sum(block * block, axis=1, keepdims=True)
+    loads[0].wait()
+    q_own = jnp.dot(scaled, qw[...], preferred_element_type=f32)
+    q_send[:, 0:q_cols] = q_own.astype(bf16)
+    q_send[:, q_cols:] = spread(sq_own, 128)
+    q_copies = [remote(q_send, q_recv.at[d], q_sem, (d,), kv_to(d)) for d in range(1, kvn)]
+    for copy in q_copies:
+        copy.start()
+    loads[1].wait()
+    loads[2].wait()
+    k_own = jnp.dot(scaled, kw[...], preferred_element_type=f32)
+    v_own = jnp.dot(scaled, vw[...], preferred_element_type=f32)
+    n_send[:, 0:k_cols] = k_own.astype(bf16)
+    n_send[:, k_cols:] = v_own.astype(bf16)
+    n_copies = [remote(n_send, n_recv.at[d], n_sem, (d,), kv_to(d)) for d in range(1, kvn)]
+    for copy in n_copies:
+        copy.start()
+    for copy in q_copies:
+        copy.wait()
+    sq_sum = sq_own
+    q_sum = q_own
+    for d in range(1, kvn):
+        sq_sum = sq_sum + gathered(q_recv[d, :, q_cols:])
+        q_sum = q_sum + q_recv[d, :, 0:q_cols].astype(f32)
+    inv_rms = lax.rsqrt(sq_sum / model + EPS)
+    scale = 1.0 / HALF**0.5
+    query = (inv_rms * q_sum).astype(bf16).astype(f32) * scale
+    low_half = lax.broadcasted_iota(jnp.int32, (rows, VDIM), 1) < HALF
+    for h in range(reps // 2):
+        piece = query[:, h * VDIM : (h + 1) * VDIM]
+        q_rows[:, 2 * h, :] = jnp.where(low_half, piece, 0.0)
+        q_rows[:, 2 * h + 1, :] = jnp.where(low_half, 0.0, piece)
+
+    columns = keys.shape[1]
+    share = reps // kv_local
+    col = lax.broadcasted_iota(jnp.int32, (reps, columns), 1)
+    row = lax.broadcasted_iota(jnp.int32, (reps, columns), 0)
+    valid = lax.rem(col, kv_local) == row // share
+    lane = lax.broadcasted_iota(jnp.int32, (reps, 128), 1)
+
+    def w_copy(g, d):
+        span = pl.ds(pl.multiple_of(g * per * reps, per * reps), per * reps)
+        return remote(w_send.at[span], w_recv.at[d, span], w_sem, (g, d), kv_to(d))
+
+    def attend(g, stat):
+        cache_copy(g, 0).wait()
+        cache_copy(g, 1).wait()
+        outs = []
+        for i in range(per):
+            b = g * per + i
+            scores = lax.dot_general(
+                q_rows[b].astype(bf16),
+                keys[b],
+                (((1,), (1,)), ((), ())),
+                preferred_element_type=f32,
+            )
+            scores = jnp.where(valid, scores, -1e30)
+            top = jnp.max(scores, axis=1, keepdims=True)
+            expo = jnp.exp(scores - top)
+            total = jnp.sum(expo, axis=1, keepdims=True)
+            outs.append(jnp.dot(expo.astype(bf16), values[b], preferred_element_type=f32))
+            stat = jnp.where(lane == b, top, stat)
+            stat = jnp.where(lane == b + 64, total, stat)
+        weighted = jnp.concatenate(outs, axis=0)
+        span = pl.ds(pl.multiple_of(g * per * reps, per * reps), per * reps)
+        w_own[span, :] = weighted
+        w_send[span, :] = weighted.astype(bf16)
+        for d in range(1, kvn):
+            w_copy(g, d).start()
+        return stat
+
+    stat = lax.fori_loop(0, groups, attend, jnp.zeros((reps, 128), f32))
+    s_send[...] = stat
+    s_copies = [remote(s_send, s_recv.at[d], s_sem, (d,), kv_to(d)) for d in range(1, kvn)]
+    for copy in s_copies:
+        copy.start()
+
+    for copy in n_copies:
+        copy.wait()
+    k_sum, v_sum = k_own, v_own
+    for d in range(1, kvn):
+        k_sum = k_sum + n_recv[d, :, 0:k_cols].astype(f32)
+        v_sum = v_sum + n_recv[d, :, k_cols:].astype(f32)
+    new_key = (inv_rms * k_sum).astype(bf16).astype(f32)
+    new_value = (inv_rms * v_sum).astype(bf16).astype(f32)
+    for r in range(reps):
+        k = r // share
+        k_rows[:, r, :] = new_key[:, k * VDIM : (k + 1) * VDIM]
+        v_rows[:, r, :] = new_value[:, k * VDIM : (k + 1) * VDIM]
+    own = jnp.zeros((reps, 128), f32)
+    for b in range(rows):
+        own = jnp.where(lane == b, jnp.sum(q_rows[b] * k_rows[b], axis=1, keepdims=True), own)
+
+    for copy in s_copies:
+        copy.wait()
+    stats = [stat] + [s_recv[d] for d in range(1, kvn)]
+    top = own
+    for part in stats:
+        top = jnp.maximum(top, part)
+    own_part = jnp.exp(own - top)
+    denom = own_part
+    factors = []
+    for part in stats:
+        factors.append(jnp.exp(part - top))
+        denom = denom + factors[-1] * pltpu.roll(part, 64, 1)
+    own_part = own_part / denom
+    factors = [factor / denom for factor in factors]
+    for g in range(groups):
+        for d in range(1, kvn):
+            w_copy(g, d).wait()
+    for b in range(rows):
+        span = slice(b * reps, (b + 1) * reps)
+        total = v_rows[b] * own_part[:, b : b + 1] + w_own[span, :] * factors[0][:, b : b + 1]
+        for d in range(1, kvn):
+            total = total + w_recv[d, span, :].astype(f32) * factors[d][:, b : b + 1]
+        att[b] = total
+
+    heads = []
+    for h in range(reps // 2):
+        diff = att[:, 2 * h, :] - lambda_ref[h] * att[:, 2 * h + 1, :]
+        mean = jnp.mean(diff * diff, axis=1, keepdims=True)
+        heads.append((diff * lax.rsqrt(mean + EPS) * gains_ref[2:3, 0:VDIM]).astype(bf16))
+    heads_out = jnp.concatenate(heads, axis=1)
+    loads[3].wait()
+    o_send[...] = jnp.dot(heads_out, ow[...], preferred_element_type=f32).astype(bf16)
+    o_copies = [remote(o_send, o_all.at[me_tp], o_sem, (d,), tp_to(d)) for d in range(1, tpn)]
+    for copy in o_copies:
+        copy.start()
+    o_all[me_tp] = o_send[...]
+    for copy in o_copies:
+        copy.wait()
+    mixed = o_all[0].astype(f32)
+    for t in range(1, tpn):
+        mixed = mixed + o_all[t].astype(f32)
+    mixed = (block + mixed).astype(bf16).astype(f32)
+    scaled2 = (mixed * gains_ref[1:2, :]).astype(bf16)
+    sq_mixed = jnp.sum(mixed * mixed, axis=1, keepdims=True)
+    m_send[...] = spread(sq_mixed, 128)
+    m_copies = [remote(m_send, m_recv.at[d], m_sem, (d,), kv_to(d)) for d in range(1, kvn)]
+    for copy in m_copies:
+        copy.start()
+
+    part = uw.shape[1] // kvn
+
+    def up_for(j):
+        span = pl.ds(pl.multiple_of(j * part, part), part)
+        return jnp.dot(scaled2, uw[:, span], preferred_element_type=f32)
+
+    loads[4].wait()
+    u_copies = []
+    for d in [kvn // 2] + [d for d in range(1, kvn) if d != kvn // 2]:
+        u_send[d] = up_for(lax.rem(me_kv + d, kvn)).astype(bf16)
+        u_copies.append(remote(u_send.at[d], u_recv.at[d], u_sem, (d,), kv_to(d)))
+        u_copies[-1].start()
+    up_sum = up_for(me_kv)
+    for copy in m_copies:
+        copy.wait()
+    for d in range(1, kvn):
+        sq_mixed = sq_mixed + gathered(m_recv[d])
+    inv_rms2 = lax.rsqrt(sq_mixed / model + EPS)
+    for copy in u_copies:
+        copy.wait()
+    for d in range(1, kvn):
+        up_sum = up_sum + u_recv[d].astype(f32)
+    hidden = jnp.square(jnp.maximum(inv_rms2 * up_sum, 0.0)).astype(bf16)
+    h_send[...] = hidden
+    h_copies = [remote(h_send, h_recv.at[d], h_sem, (d,), kv_to(d)) for d in range(1, kvn)]
+    for copy in h_copies:
+        copy.start()
+
+    def down_for(block_of, j):
+        span = pl.ds(pl.multiple_of(j * part, part), part)
+        return jnp.dot(block_of, dw[span, :], preferred_element_type=f32)
+
+    loads[5].wait()
+    down = down_for(hidden, me_kv)
+    for d in sorted(range(1, kvn), key=lambda d: min(d, kvn - d)):
+        h_copies[d - 1].wait()
+        down = down + down_for(h_recv[d], lax.rem(me_kv + kvn - d, kvn))
+    for t in range(tpn):
+        d_send[t] = down[:, t * width : (t + 1) * width].astype(bf16)
+    att_out = [
+        remote(d_send.at[lax.rem(me_tp + d, tpn)], d_recv.at[d], d_sem, (d,), tp_to(d))
+        for d in range(1, tpn)
+    ]
+    for copy in att_out:
+        copy.start()
+    result = jnp.zeros((rows, width), f32)
+    for t in range(tpn):
+        here = slice(t * width, (t + 1) * width)
+        result = jnp.where(me_tp == t, mixed[:, here] + down[:, here], result)
+    for copy in att_out:
+        copy.wait()
+    for d in range(1, tpn):
+        result = result + d_recv[d].astype(f32)
+    out_ref[...] = result.astype(bf16)
+
+
+def fused_body(
+    kvn,
+    tpn,
+    residual,
+    cache_keys,
+    cache_values,
+    norm_gain,
+    query_weight,
+    key_weight,
+    value_weight,
+    head_lambda,
+    head_gain,
+    out_weight,
+    mixer_gain,
+    up_weight,
+    down_weight,
+):
+    f32 = jnp.float32
+    bf16 = jnp.bfloat16
+    rows, width = residual.shape
+    positions, kv_local = cache_keys.shape[1:3]
+    depth, q_cols = query_weight.shape
+    k_cols = key_weight.shape[1]
+    part = up_weight.shape[1] // kvn
+    reps = q_cols // VDIM * 2
+    groups = 4
+    keys = cache_keys.reshape(rows, positions * kv_local, VDIM)
+    values = cache_values.reshape(rows, positions * kv_local, VDIM)
+    gains = jnp.stack(
+        [norm_gain, mixer_gain, jnp.pad(head_gain, (0, depth - VDIM))]
+    ).astype(f32)
+    vmem = pl.BlockSpec(memory_space=pltpu.VMEM)
+    away = pl.BlockSpec(memory_space=pl.ANY)
+    big = (keys, values, query_weight, key_weight, value_weight, out_weight, up_weight, down_weight)
+    V = pltpu.VMEM
+    dma = pltpu.SemaphoreType.DMA
+    scratch = [V(a.shape, a.dtype) for a in big] + [
+        V((tpn, rows, width), bf16),
+        V((rows, q_cols + 128), bf16),
+        V((kvn, rows, q_cols + 128), bf16),
+        V((rows, 2 * k_cols), bf16),
+        V((kvn, rows, 2 * k_cols), bf16),
+        V((rows, reps, VDIM), f32),
+        V((rows, reps, VDIM), f32),
+        V((rows, reps, VDIM), f32),
+        V((rows * reps, VDIM), f32),
+        V((rows * reps, VDIM), bf16),
+        V((kvn, rows * reps, VDIM), bf16),
+        V((reps, 128), f32),
+        V((kvn, reps, 128), f32),
+        V((rows, reps, VDIM), f32),
+        V((tpn, rows, depth), bf16),
+        V((rows, depth), bf16),
+        V((rows, 128), bf16),
+        V((kvn, rows, 128), bf16),
+        V((kvn, rows, part), bf16),
+        V((kvn, rows, part), bf16),
+        V((rows, part), bf16),
+        V((kvn, rows, part), bf16),
+        V((tpn, rows, width), bf16),
+        V((tpn, rows, width), bf16),
+        dma((6,)),
+        dma((groups, 2)),
+        dma((2, tpn)),
+        dma((2, kvn)),
+        dma((2, kvn)),
+        dma((2, groups, kvn)),
+        dma((2, kvn)),
+        dma((2, tpn)),
+        dma((2, kvn)),
+        dma((2, kvn)),
+        dma((2, kvn)),
+        dma((2, tpn)),
+    ]
+    return pl.pallas_call(
+        functools.partial(layer_kernel, (kvn, tpn, kv_local, groups)),
+        out_shape=jax.ShapeDtypeStruct((rows, width), bf16),
+        in_specs=[vmem, vmem, pl.BlockSpec(memory_space=pltpu.SMEM)] + [away] * 8,
+        out_specs=vmem,
+        scratch_shapes=scratch,
+        compiler_params=pltpu.CompilerParams(
+            collective_id=0, has_side_effects=True, vmem_limit_bytes=60 * 2**20
+        ),
+        name="layer",
+    )(residual, gains, head_lambda, *big)
+
+
+def fits(mesh):
+    kvn, tpn = mesh.shape["kv"], mesh.shape["tp"]
+    heads = HEADS // tpn
+    return D // (kvn * tpn) % 128 == 0 and heads * 2 % 8 == 0 and KV_HEADS // tpn > 1
+
+
 def solution(mesh):
+    kvn, tpn = mesh.shape["kv"], mesh.shape["tp"]
+    body = functools.partial(fused_body, kvn, tpn) if fits(mesh) else plain_body
     in_specs = (
         P("grp", ("kv", "tp")),
         P("grp", "kv", "tp", None),

time: 214 us -> 48.2 us (0.23)
  blocking collectives: 77.6 us -> 0 us
  waiting for transfers between devices: 60.5 us -> 0 us
  Pallas kernels: 0 us -> 43.9 us
  matrix products: 26.7 us -> 0 us
  local copies, waits for them, and re-layouts: 25 us -> 3.33 us
  between operations: 13.3 us -> 0.01 us
  other arithmetic: 9.24 us -> 0.61 us
    all_gather x6 -> x0, blocking collectives: 65.8 us -> none  [the longest x3 40.8 us: joined(): everything = jax.tree.map(lambda part: lax.all_gather(part, axis), shard)]
    reduce_scatter x3 -> x0, waiting for transfers between devices: 46 us -> none  [the longest x1 19.9 us: body(): lax.psum_scatter(projected, 'tp', scatter_dimension=1, tiled=True)]
    pallas_call x0 -> x1, Pallas kernels: none -> 43.9 us  [fused_body(): pl.pallas_call(functools.partial(layer_kernel, (kvn, tpn, kv_local, group...]
    dot_general x9 -> x0, matrix products: 26.7 us -> none  [the longest x1 5.28 us: body(): up_part = jnp.dot(scaled2, up_weight, preferred_element_type=f32)]
    unnamed x9 -> x1, local copies, waits for them, and re-layouts: 21.2 us -> 1.3 us
    psum x1 -> x0, waiting for transfers between devices: 14.4 us -> none  [body(): lax.psum((q_part, k_part, v_part, sq_part), 'kv')]
    psum x1 -> x0, blocking collectives: 11.8 us -> none  [body(): sq_total = lax.psum(sq_mixed, 'kv')]
    convert_element_type x7 -> x1, other arithmetic: 5.37 us -> 0.61 us  [fused_body(): gains = jnp.stack([norm_gain, mixer_gain, jnp.pad(head_gain, (0, depth -...]
  transfers between devices with their start and end apart: 4 -> 0, of which waited for: 4 -> 0; matrix products, arithmetic and copies ran while one was open for 10% -> 0% of each run, Pallas kernels for 0% -> 0%
where the time goes in v1:
time: 48.2 us; the launch traced here: 47.8 us
  Pallas kernels  43.9 us (91%)
  local copies, waits for them, and re-layouts  3.33 us (7%)
  other arithmetic  0.61 us (1%)
    pallas_call x1, Pallas kernels, fused_body(): pl.pallas_call(functools.partial(layer_kernel, (kvn, tpn, kv_local, group...  43.9 us
    another operation x3, local copies, waits for them, and re-layouts, fused_body(): jnp.stack([norm_gain, mixer_gain, jnp.pad(head_gain, (0, depth - VDIM))])  1.38 us
    unnamed x1, local copies, waits for them, and re-layouts  1.3 us

profile of v1, /device:TPU:0, one launch (start us, length us, event | category | flops | bytes accessed | tf_op | source)
XLA Modules:
  0.0 47.8 jit_solution(16357722634439407822)
XLA Ops:
  0.0 0.7 %pad.4 = bf16[1024]{0:T(1024)(128)(2,1)S(1)} pad(bf16[128]{0:T(256)(128)(2,1)} %param.21, bf16[]{:T(256)} %constant.2.clone.1), padding=0_896 | pad | bytes 2306 | tf_op jit(solution)/shard_map/jit(_pad)/pad | solution.py:479
  0.7 0.7 %stack.12 = bf16[1,1024]{1,0:T(2,128)(2,1)S(1)} reshape(bf16[1024]{0:T(1024)(128)(2,1)} %param.16) | data formatting | bytes 4096 | tf_op jit(solution)/shard_map/stack | solution.py:478
  1.4 0.7 %stack.13 = bf16[1,1024]{1,0:T(2,128)(2,1)S(1)} reshape(bf16[1024]{0:T(1024)(128)(2,1)} %param.23) | data formatting | bytes 4096 | tf_op jit(solution)/shard_map/stack | solution.py:478
  2.0 0.6 %maximum_convert_fusion.gains_ref = f32[3,1024]{1,0:T(4,128)} fusion(bf16[1,1024]{1,0:T(2,128)(2,1)S(1)} %stack.14, bf16[1,1024]{1,0:T(2,128)(2,1)S(1)} %stack.13, bf16[1,1024]{1,0:T(2,128)(2,1)S(1)} %stack.12), kind=kLoop, calls=%fused_computation | loop fusion | flops 18432 | bytes 18432 | tf_op jit(solution)/shard_map/convert_element_type | solution.py:480
  2.7 43.9 %layer.1 = bf16[16,256]{1,0:T(8,128)(2,1)} custom-call(bf16[16,256]{1,0:T(8,128)(2,1)} %residual_ref.1, f32[3,1024]{1,0:T(4,128)} %maximum_convert_fusion.gains_ref, f32[4]{0:T(128)} %lambda_ref.1, bf16[16,2048,128]{2,1,0:T(8,128)(2,1)} %bitcast.2, bf16[16,2048,128]{2,1,0:T(8,128)(2,1)} %bitcast.3, bf16[1024,512]{1,0:T(8,128)(2,1)} %qw_hbm.1, ...), custom_call_target="tpu_custom_call" | custom-call | tf_op jit(solution)/shard_map/layer/pallas_call | solution.py:524
  46.5 1.3 %copy.15 = bf16[16,256]{1,0:T(8,128)(2,1)} copy(bf16[16,256]{1,0:T(8,128)(2,1)} %layer.1) | data formatting | bytes 16384
  (1 shorter events, 0.0 us)

commit v2 on v1

--- a/solution.py
+++ b/solution.py
@@ -126,10 +126,21 @@
     return pair[:, 0:1] + pair[:, half : half + 1]
 
 
+def partner(index, distance):
+    bit = 1
+    while bit <= distance:
+        if distance & bit:
+            index = index + bit - 2 * bit * ((index // bit) % 2)
+        bit *= 2
+    return index
+
+
 def layer_kernel(
     dims,
     residual_ref,
-    gains_ref,
+    norm_ref,
+    mixer_ref,
+    head_ref,
     lambda_ref,
     keys_hbm,
     values_hbm,
@@ -151,6 +162,8 @@
     x_all,
     q_send,
     q_recv,
+    r_send,
+    r_recv,
     n_send,
     n_recv,
     q_rows,
@@ -176,6 +189,7 @@
     cache_sem,
     x_sem,
     q_sem,
+    r_sem,
     n_sem,
     w_sem,
     s_sem,
@@ -198,6 +212,8 @@
     me_kv = lax.axis_index("kv")
     me_tp = lax.axis_index("tp")
 
+    far_kv = list(reversed(range(1, kvn)))
+    far_tp = list(reversed(range(1, tpn)))
     loads = []
     for index, (src, dst) in enumerate(((qw_hbm, qw), (kw_hbm, kw), (vw_hbm, vw))):
         loads.append(pltpu.make_async_copy(src, dst, load_sem.at[index]))
@@ -211,15 +227,11 @@
     for g in range(groups):
         cache_copy(g, 0).start()
         cache_copy(g, 1).start()
-    for index, (src, dst) in enumerate(((ow_hbm, ow), (uw_hbm, uw), (dw_hbm, dw))):
-        loads.append(pltpu.make_async_copy(src, dst, load_sem.at[3 + index]))
-        loads[-1].start()
-
     def kv_to(d):
-        return {"kv": lax.rem(me_kv + d, kvn)}
+        return {"kv": partner(me_kv, d)}
 
     def tp_to(d):
-        return {"tp": lax.rem(me_tp + d, tpn)}
+        return {"tp": partner(me_tp, d)}
 
     def remote(src, dst, sems, index, target):
         return pltpu.make_async_remote_copy(
@@ -239,22 +251,28 @@
     pl.semaphore_wait(barrier, tpn + kvn - 2)
 
     x_copies = [
-        remote(residual_ref, x_all.at[me_tp], x_sem, (d,), tp_to(d)) for d in range(1, tpn)
+        remote(residual_ref, x_all.at[me_tp], x_sem, (d,), tp_to(d)) for d in reversed(range(1, tpn))
     ]
     for copy in x_copies:
         copy.start()
     x_all[me_tp] = residual_ref[...]
     for copy in x_copies:
         copy.wait()
+    for index, (src, dst) in enumerate(((ow_hbm, ow), (uw_hbm, uw), (dw_hbm, dw))):
+        loads.append(pltpu.make_async_copy(src, dst, load_sem.at[3 + index]))
+        loads[-1].start()
 
     block = jnp.concatenate([x_all[t] for t in range(tpn)], axis=1).astype(f32)
-    scaled = (block * gains_ref[0:1, :]).astype(bf16)
+    scaled = (block * norm_ref[...].astype(f32)[None, :]).astype(bf16)
     sq_own = jnp.sum(block * block, axis=1, keepdims=True)
+    r_send[...] = spread(sq_own, 128)
+    r_copies = [remote(r_send, r_recv.at[d], r_sem, (d,), kv_to(d)) for d in far_kv]
+    for copy in r_copies:
+        copy.start()
     loads[0].wait()
     q_own = jnp.dot(scaled, qw[...], preferred_element_type=f32)
-    q_send[:, 0:q_cols] = q_own.astype(bf16)
-    q_send[:, q_cols:] = spread(sq_own, 128)
-    q_copies = [remote(q_send, q_recv.at[d], q_sem, (d,), kv_to(d)) for d in range(1, kvn)]
+    q_send[...] = q_own.astype(bf16)
+    q_copies = [remote(q_send, q_recv.at[d], q_sem, (d,), kv_to(d)) for d in far_kv]
     for copy in q_copies:
         copy.start()
     loads[1].wait()
@@ -263,16 +281,18 @@
     v_own = jnp.dot(scaled, vw[...], preferred_element_type=f32)
     n_send[:, 0:k_cols] = k_own.astype(bf16)
     n_send[:, k_cols:] = v_own.astype(bf16)
-    n_copies = [remote(n_send, n_recv.at[d], n_sem, (d,), kv_to(d)) for d in range(1, kvn)]
+    for copy in r_copies:
+        copy.wait()
+    for copy in q_copies:
+        copy.wait()
+    n_copies = [remote(n_send, n_recv.at[d], n_sem, (d,), kv_to(d)) for d in far_kv]
     for copy in n_copies:
         copy.start()
-    for copy in q_copies:
-        copy.wait()
     sq_sum = sq_own
     q_sum = q_own
     for d in range(1, kvn):
-        sq_sum = sq_sum + gathered(q_recv[d, :, q_cols:])
-        q_sum = q_sum + q_recv[d, :, 0:q_cols].astype(f32)
+        sq_sum = sq_sum + gathered(r_recv[d])
+        q_sum = q_sum + q_recv[d].astype(f32)
     inv_rms = lax.rsqrt(sq_sum / model + EPS)
     scale = 1.0 / HALF**0.5
     query = (inv_rms * q_sum).astype(bf16).astype(f32) * scale
@@ -284,45 +304,66 @@
 
     columns = keys.shape[1]
     share = reps // kv_local
-    col = lax.broadcasted_iota(jnp.int32, (reps, columns), 1)
-    row = lax.broadcasted_iota(jnp.int32, (reps, columns), 0)
-    valid = lax.rem(col, kv_local) == row // share
+    col = lax.broadcasted_iota(jnp.int32, (2 * reps, columns), 1)
+    row = lax.broadcasted_iota(jnp.int32, (2 * reps, columns), 0)
+    valid = lax.rem(col, kv_local) == lax.rem(row, reps) // share
     lane = lax.broadcasted_iota(jnp.int32, (reps, 128), 1)
 
-    def w_copy(g, d):
-        span = pl.ds(pl.multiple_of(g * per * reps, per * reps), per * reps)
-        return remote(w_send.at[span], w_recv.at[d, span], w_sem, (g, d), kv_to(d))
-
-    def attend(g, stat):
+    def w_copy(p, d):
+        span = slice(p * 2 * reps, (p + 1) * 2 * reps)
+        return remote(w_send.at[span], w_recv.at[d, span], w_sem, (p, d), kv_to(d))
+
+    def scores_of(p):
+        b = 2 * p
+        none = jnp.zeros((reps, VDIM), f32)
+        both = jnp.concatenate(
+            [
+                jnp.concatenate([q_rows[b], none], axis=1),
+                jnp.concatenate([none, q_rows[b + 1]], axis=1),
+            ],
+            axis=0,
+        ).astype(bf16)
+        return lax.dot_general(
+            both,
+            jnp.concatenate([keys[b], keys[b + 1]], axis=1),
+            (((1,), (1,)), ((), ())),
+            preferred_element_type=f32,
+        )
+
+    for g in range(groups):
         cache_copy(g, 0).wait()
         cache_copy(g, 1).wait()
+    stat = jnp.zeros((reps, 128), f32)
+    pairs = rows // 2
+    scores = scores_of(0)
+    for p in range(pairs):
+        b = 2 * p
+        later = scores_of(p + 1) if p + 1 < pairs else None
+        scores = jnp.where(valid, scores, -1e30)
+        top = jnp.max(scores, axis=1, keepdims=True)
+        expo = jnp.exp(scores - top)
+        total = jnp.sum(expo, axis=1, keepdims=True)
+        product = jnp.dot(
+            expo.astype(bf16),
+            jnp.concatenate([values[b], values[b + 1]], axis=1),
+            preferred_element_type=f32,
+        )
         outs = []
-        for i in range(per):
-            b = g * per + i
-            scores = lax.dot_general(
-                q_rows[b].astype(bf16),
-                keys[b],
-                (((1,), (1,)), ((), ())),
-                preferred_element_type=f32,
-            )
-            scores = jnp.where(valid, scores, -1e30)
-            top = jnp.max(scores, axis=1, keepdims=True)
-            expo = jnp.exp(scores - top)
-            total = jnp.sum(expo, axis=1, keepdims=True)
-            outs.append(jnp.dot(expo.astype(bf16), values[b], preferred_element_type=f32))
-            stat = jnp.where(lane == b, top, stat)
-            stat = jnp.where(lane == b + 64, total, stat)
+        for side in range(2):
+            here = slice(side * reps, (side + 1) * reps)
+            outs.append(product[here, side * VDIM : (side + 1) * VDIM])
+            stat = jnp.where(lane == b + side, top[here], stat)
+            stat = jnp.where(lane == b + side + 64, total[here], stat)
         weighted = jnp.concatenate(outs, axis=0)
-        span = pl.ds(pl.multiple_of(g * per * reps, per * reps), per * reps)
+        span = slice(p * 2 * reps, (p + 1) * 2 * reps)
         w_own[span, :] = weighted
         w_send[span, :] = weighted.astype(bf16)
-        for d in range(1, kvn):
-            w_copy(g, d).start()
-        return stat
-
-    stat = lax.fori_loop(0, groups, attend, jnp.zeros((reps, 128), f32))
+        for d in far_kv:
+            w_copy(p, d).start()
+        scores = later
+
     s_send[...] = stat
-    s_copies = [remote(s_send, s_recv.at[d], s_sem, (d,), kv_to(d)) for d in range(1, kvn)]
+    s_copies = [remote(s_send, s_recv.at[d], s_sem, (d,), kv_to(d)) for d in far_kv]
     for copy in s_copies:
         copy.start()
 
@@ -356,9 +397,9 @@
         denom = denom + factors[-1] * pltpu.roll(part, 64, 1)
     own_part = own_part / denom
     factors = [factor / denom for factor in factors]
-    for g in range(groups):
-        for d in range(1, kvn):
-            w_copy(g, d).wait()
+    for p in range(pairs):
+        for d in far_kv:
+            w_copy(p, d).wait()
     for b in range(rows):
         span = slice(b * reps, (b + 1) * reps)
         total = v_rows[b] * own_part[:, b : b + 1] + w_own[span, :] * factors[0][:, b : b + 1]
@@ -370,11 +411,11 @@
     for h in range(reps // 2):
         diff = att[:, 2 * h, :] - lambda_ref[h] * att[:, 2 * h + 1, :]
         mean = jnp.mean(diff * diff, axis=1, keepdims=True)
-        heads.append((diff * lax.rsqrt(mean + EPS) * gains_ref[2:3, 0:VDIM]).astype(bf16))
+        heads.append((diff * lax.rsqrt(mean + EPS) * head_ref[...].astype(f32)[None, :]).astype(bf16))
     heads_out = jnp.concatenate(heads, axis=1)
     loads[3].wait()
     o_send[...] = jnp.dot(heads_out, ow[...], preferred_element_type=f32).astype(bf16)
-    o_copies = [remote(o_send, o_all.at[me_tp], o_sem, (d,), tp_to(d)) for d in range(1, tpn)]
+    o_copies = [remote(o_send, o_all.at[me_tp], o_sem, (d,), tp_to(d)) for d in far_tp]
     for copy in o_copies:
         copy.start()
     o_all[me_tp] = o_send[...]
@@ -384,55 +425,68 @@
     for t in range(1, tpn):
         mixed = mixed + o_all[t].astype(f32)
     mixed = (block + mixed).astype(bf16).astype(f32)
-    scaled2 = (mixed * gains_ref[1:2, :]).astype(bf16)
+    scaled2 = (mixed * mixer_ref[...].astype(f32)[None, :]).astype(bf16)
     sq_mixed = jnp.sum(mixed * mixed, axis=1, keepdims=True)
     m_send[...] = spread(sq_mixed, 128)
-    m_copies = [remote(m_send, m_recv.at[d], m_sem, (d,), kv_to(d)) for d in range(1, kvn)]
+    m_copies = [remote(m_send, m_recv.at[d], m_sem, (d,), kv_to(d)) for d in far_kv]
     for copy in m_copies:
         copy.start()
 
     part = uw.shape[1] // kvn
 
-    def up_for(j):
-        span = pl.ds(pl.multiple_of(j * part, part), part)
+    piece = part // 2
+
+    def up_for(j, half):
+        span = pl.ds(pl.multiple_of(j * part + half * piece, piece), piece)
         return jnp.dot(scaled2, uw[:, span], preferred_element_type=f32)
 
     loads[4].wait()
-    u_copies = []
-    for d in [kvn // 2] + [d for d in range(1, kvn) if d != kvn // 2]:
-        u_send[d] = up_for(lax.rem(me_kv + d, kvn)).astype(bf16)
-        u_copies.append(remote(u_send.at[d], u_recv.at[d], u_sem, (d,), kv_to(d)))
-        u_copies[-1].start()
-    up_sum = up_for(me_kv)
+    u_copies = {}
+    for half in range(2):
+        for d in far_kv:
+            u_send[half, d] = up_for(partner(me_kv, d), half).astype(bf16)
+            u_copies[half, d] = remote(
+                u_send.at[half, d], u_recv.at[half, d], u_sem, (half, d), kv_to(d)
+            )
+            u_copies[half, d].start()
+    up_own = [up_for(me_kv, half) for half in range(2)]
     for copy in m_copies:
         copy.wait()
     for d in range(1, kvn):
         sq_mixed = sq_mixed + gathered(m_recv[d])
     inv_rms2 = lax.rsqrt(sq_mixed / model + EPS)
-    for copy in u_copies:
-        copy.wait()
-    for d in range(1, kvn):
-        up_sum = up_sum + u_recv[d].astype(f32)
-    hidden = jnp.square(jnp.maximum(inv_rms2 * up_sum, 0.0)).astype(bf16)
-    h_send[...] = hidden
-    h_copies = [remote(h_send, h_recv.at[d], h_sem, (d,), kv_to(d)) for d in range(1, kvn)]
-    for copy in h_copies:
-        copy.start()
-
-    def down_for(block_of, j):
-        span = pl.ds(pl.multiple_of(j * part, part), part)
+    h_copies = {}
+    own_hidden = []
+    for half in range(2):
+        for d in far_kv:
+            u_copies[half, d].wait()
+        up_sum = up_own[half]
+        for d in range(1, kvn):
+            up_sum = up_sum + u_recv[half, d].astype(f32)
+        hidden = jnp.square(jnp.maximum(inv_rms2 * up_sum, 0.0)).astype(bf16)
+        own_hidden.append(hidden)
+        h_send[half] = hidden
+        for d in far_kv:
+            h_copies[half, d] = remote(
+                h_send.at[half], h_recv.at[half, d], h_sem, (half, d), kv_to(d)
+            )
+            h_copies[half, d].start()
+
+    def down_for(block_of, j, half):
+        span = pl.ds(pl.multiple_of(j * part + half * piece, piece), piece)
         return jnp.dot(block_of, dw[span, :], preferred_element_type=f32)
 
     loads[5].wait()
-    down = down_for(hidden, me_kv)
-    for d in sorted(range(1, kvn), key=lambda d: min(d, kvn - d)):
-        h_copies[d - 1].wait()
-        down = down + down_for(h_recv[d], lax.rem(me_kv + kvn - d, kvn))
+    down = down_for(own_hidden[0], me_kv, 0) + down_for(own_hidden[1], me_kv, 1)
+    for half in range(2):
+        for d in range(1, kvn):
+            h_copies[half, d].wait()
+            down = down + down_for(h_recv[half, d], partner(me_kv, d), half)
     for t in range(tpn):
         d_send[t] = down[:, t * width : (t + 1) * width].astype(bf16)
     att_out = [
-        remote(d_send.at[lax.rem(me_tp + d, tpn)], d_recv.at[d], d_sem, (d,), tp_to(d))
-        for d in range(1, tpn)
+        remote(d_send.at[partner(me_tp, d)], d_recv.at[d], d_sem, (d,), tp_to(d))
+        for d in reversed(range(1, tpn))
     ]
     for copy in att_out:
         copy.start()
@@ -475,9 +529,6 @@
     groups = 4
     keys = cache_keys.reshape(rows, positions * kv_local, VDIM)
     values = cache_values.reshape(rows, positions * kv_local, VDIM)
-    gains = jnp.stack(
-        [norm_gain, mixer_gain, jnp.pad(head_gain, (0, depth - VDIM))]
-    ).astype(f32)
     vmem = pl.BlockSpec(memory_space=pltpu.VMEM)
     away = pl.BlockSpec(memory_space=pl.ANY)
     big = (keys, values, query_weight, key_weight, value_weight, out_weight, up_weight, down_weight)
@@ -485,8 +536,10 @@
     dma = pltpu.SemaphoreType.DMA
     scratch = [V(a.shape, a.dtype) for a in big] + [
         V((tpn, rows, width), bf16),
-        V((rows, q_cols + 128), bf16),
-        V((kvn, rows, q_cols + 128), bf16),
+        V((rows, q_cols), bf16),
+        V((kvn, rows, q_cols), bf16),
+        V((rows, 128), bf16),
+        V((kvn, rows, 128), bf16),
         V((rows, 2 * k_cols), bf16),
         V((kvn, rows, 2 * k_cols), bf16),
         V((rows, reps, VDIM), f32),
@@ -502,10 +555,10 @@
         V((rows, depth), bf16),
         V((rows, 128), bf16),
         V((kvn, rows, 128), bf16),
-        V((kvn, rows, part), bf16),
-        V((kvn, rows, part), bf16),
-        V((rows, part), bf16),
-        V((kvn, rows, part), bf16),
+        V((2, kvn, rows, part // 2), bf16),
+        V((2, kvn, rows, part // 2), bf16),
+        V((2, rows, part // 2), bf16),
+        V((2, kvn, rows, part // 2), bf16),
         V((tpn, rows, width), bf16),
         V((tpn, rows, width), bf16),
         dma((6,)),
@@ -513,31 +566,33 @@
         dma((2, tpn)),
         dma((2, kvn)),
         dma((2, kvn)),
-        dma((2, groups, kvn)),
+        dma((2, kvn)),
+        dma((2, rows // 2, kvn)),
         dma((2, kvn)),
         dma((2, tpn)),
         dma((2, kvn)),
-        dma((2, kvn)),
-        dma((2, kvn)),
+        dma((2, 2, kvn)),
+        dma((2, 2, kvn)),
         dma((2, tpn)),
     ]
     return pl.pallas_call(
         functools.partial(layer_kernel, (kvn, tpn, kv_local, groups)),
-        out_shape=jax.ShapeDtypeStruct((rows, width), bf16),
-        in_specs=[vmem, vmem, pl.BlockSpec(memory_space=pltpu.SMEM)] + [away] * 8,
+        out_shape=pltpu.VMEM((rows, width), bf16),
+        in_specs=[vmem] * 4 + [pl.BlockSpec(memory_space=pltpu.SMEM)] + [away] * 8,
         out_specs=vmem,
         scratch_shapes=scratch,
         compiler_params=pltpu.CompilerParams(
             collective_id=0, has_side_effects=True, vmem_limit_bytes=60 * 2**20
         ),
         name="layer",
-    )(residual, gains, head_lambda, *big)
+    )(residual, norm_gain, mixer_gain, head_gain, head_lambda, *big)
 
 
 def fits(mesh):
     kvn, tpn = mesh.shape["kv"], mesh.shape["tp"]
     heads = HEADS // tpn
-    return D // (kvn * tpn) % 128 == 0 and heads * 2 % 8 == 0 and KV_HEADS // tpn > 1
+    paired = kvn & (kvn - 1) == 0 and tpn & (tpn - 1) == 0
+    return paired and D // (kvn * tpn) % 128 == 0 and heads * 2 % 8 == 0 and KV_HEADS // tpn > 1
 
 
 def solution(mesh):

time: 48.2 us -> 40 us (0.83)
  Pallas kernels: 43.9 us -> 39.2 us
  local copies, waits for them, and re-layouts: 3.33 us -> 0.6 us
  other arithmetic: 0.61 us -> 0 us
    pallas_call x1, Pallas kernels: 43.9 us -> 39.2 us  [fused_body(): pl.pallas_call(functools.partial(layer_kernel, (kvn, tpn, kv_local, group...]
    another operation x3 -> x0, local copies, waits for them, and re-layouts: 1.38 us -> none  [fused_body(): jnp.stack([norm_gain, mixer_gain, jnp.pad(head_gain, (0, depth - VDIM))])]
    unnamed x1, local copies, waits for them, and re-layouts: 1.3 us -> 0.6 us
    pad x1 -> x0, local copies, waits for them, and re-layouts: 0.66 us -> none  [fused_body(): jnp.pad(head_gain, (0, depth - VDIM))]
    convert_element_type x1 -> x0, other arithmetic: 0.61 us -> none  [fused_body(): gains = jnp.stack([norm_gain, mixer_gain, jnp.pad(head_gain, (0, depth -...]
where the time goes in v2:
time: 40 us; the launch traced here: 39.8 us
  Pallas kernels  39.2 us (98%)
  local copies, waits for them, and re-layouts  0.6 us (2%)
    pallas_call x1, Pallas kernels, fused_body(): pl.pallas_call(functools.partial(layer_kernel, (kvn, tpn, kv_local, group...  39.2 us

profile of v2, /device:TPU:0, one launch (start us, length us, event | category | flops | bytes accessed | tf_op | source)
XLA Modules:
  0.0 39.8 jit_solution(12014038615080915100)
XLA Ops:
  0.0 39.2 %layer.1 = bf16[16,256]{1,0:T(8,128)(2,1)S(1)} custom-call(bf16[16,256]{1,0:T(8,128)(2,1)} %residual_ref.1, bf16[1024]{0:T(1024)(128)(2,1)} %norm_ref.1, bf16[1024]{0:T(1024)(128)(2,1)} %mixer_ref.1, bf16[128]{0:T(256)(128)(2,1)} %head_ref.1, f32[4]{0:T(128)} %lambda_ref.1, bf16[16,2048,128]{2,1,0:T(8,128)(2,1)} %bitcast.2, bf16[16,2048,128]{2,1,0:T(8,128)(2,1)} %bitcast.3, ...), custom_call_target="tpu_custom_call" | custom-call | tf_op jit(solution)/shard_map/layer/pallas_call | solution.py:578
  39.2 0.6 %copy.15 = bf16[16,256]{1,0:T(8,128)(2,1)} copy(bf16[16,256]{1,0:T(8,128)(2,1)S(1)} %layer.1) | data formatting | bytes 16384

commit v3 on v2

--- a/solution.py
+++ b/solution.py
@@ -138,9 +138,9 @@
 def layer_kernel(
     dims,
     residual_ref,
-    norm_ref,
-    mixer_ref,
-    head_ref,
+    norm_hbm,
+    mixer_hbm,
+    head_hbm,
     lambda_ref,
     keys_hbm,
     values_hbm,
@@ -151,6 +151,9 @@
     uw_hbm,
     dw_hbm,
     out_ref,
+    norm_ref,
+    mixer_ref,
+    head_ref,
     keys,
     values,
     qw,
@@ -202,8 +205,7 @@
     f32 = jnp.float32
     bf16 = jnp.bfloat16
     kvn, tpn, kv_local, groups = dims
-    rows = residual_ref.shape[0]
-    width = residual_ref.shape[1]
+    rows, width = residual_ref.shape
     q_cols = qw.shape[1]
     k_cols = kw.shape[1]
     reps = q_cols // VDIM * 2
@@ -217,16 +219,24 @@
     loads = []
     for index, (src, dst) in enumerate(((qw_hbm, qw), (kw_hbm, kw), (vw_hbm, vw))):
         loads.append(pltpu.make_async_copy(src, dst, load_sem.at[index]))
-        loads[-1].start()
+    small = []
+    for index, (src, dst) in enumerate(
+        (
+            (residual_ref, x_all.at[me_tp]),
+            (norm_hbm, norm_ref),
+            (mixer_hbm, mixer_ref),
+            (head_hbm, head_ref),
+        )
+    ):
+        small.append(pltpu.make_async_copy(src, dst, load_sem.at[6 + index]))
+    for copy in small + loads:
+        copy.start()
 
     def cache_copy(g, which):
         src, dst = ((keys_hbm, keys), (values_hbm, values))[which]
         span = pl.ds(g * per, per)
         return pltpu.make_async_copy(src.at[span], dst.at[span], cache_sem.at[g, which])
 
-    for g in range(groups):
-        cache_copy(g, 0).start()
-        cache_copy(g, 1).start()
     def kv_to(d):
         return {"kv": partner(me_kv, d)}
 
@@ -244,20 +254,30 @@
         )
 
     barrier = pltpu.get_barrier_semaphore()
+    mesh_id = pl.DeviceIdType.MESH
     for d in range(1, tpn):
-        pl.semaphore_signal(barrier, 1, device_id=tp_to(d), device_id_type=pl.DeviceIdType.MESH)
-    for d in range(1, kvn):
-        pl.semaphore_signal(barrier, 1, device_id=kv_to(d), device_id_type=pl.DeviceIdType.MESH)
-    pl.semaphore_wait(barrier, tpn + kvn - 2)
+        pl.semaphore_signal(barrier, 1, device_id=tp_to(d), device_id_type=mesh_id)
+    pl.semaphore_wait(barrier, tpn - 1 + me_kv)
+    for d in far_kv:
+        pl.semaphore_signal(barrier, 1, device_id=kv_to(d), device_id_type=mesh_id)
 
     x_copies = [
         remote(residual_ref, x_all.at[me_tp], x_sem, (d,), tp_to(d)) for d in reversed(range(1, tpn))
     ]
     for copy in x_copies:
         copy.start()
-    x_all[me_tp] = residual_ref[...]
+    for g in range(groups):
+        cache_copy(g, 0).start()
+        cache_copy(g, 1).start()
+    for copy in small:
+        copy.wait()
     for copy in x_copies:
         copy.wait()
+
+    @pl.when(me_kv < kvn - 1)
+    def _():
+        pl.semaphore_wait(barrier, kvn - 1 - me_kv)
+
     for index, (src, dst) in enumerate(((ow_hbm, ow), (uw_hbm, uw), (dw_hbm, dw))):
         loads.append(pltpu.make_async_copy(src, dst, load_sem.at[3 + index]))
         loads[-1].start()
@@ -534,7 +554,7 @@
     big = (keys, values, query_weight, key_weight, value_weight, out_weight, up_weight, down_weight)
     V = pltpu.VMEM
     dma = pltpu.SemaphoreType.DMA
-    scratch = [V(a.shape, a.dtype) for a in big] + [
+    scratch = [V(a.shape, a.dtype) for a in (norm_gain, mixer_gain, head_gain) + big] + [
         V((tpn, rows, width), bf16),
         V((rows, q_cols), bf16),
         V((kvn, rows, q_cols), bf16),
@@ -561,7 +581,7 @@
         V((2, kvn, rows, part // 2), bf16),
         V((tpn, rows, width), bf16),
         V((tpn, rows, width), bf16),
-        dma((6,)),
+        dma((10,)),
         dma((groups, 2)),
         dma((2, tpn)),
         dma((2, kvn)),
@@ -578,7 +598,7 @@
     return pl.pallas_call(
         functools.partial(layer_kernel, (kvn, tpn, kv_local, groups)),
         out_shape=pltpu.VMEM((rows, width), bf16),
-        in_specs=[vmem] * 4 + [pl.BlockSpec(memory_space=pltpu.SMEM)] + [away] * 8,
+        in_specs=[away] * 4 + [pl.BlockSpec(memory_space=pltpu.SMEM)] + [away] * 8,
         out_specs=vmem,
         scratch_shapes=scratch,
         compiler_params=pltpu.CompilerParams(

time: 40 us -> 39.4 us (0.985)
  Pallas kernels: 39.2 us -> 38.6 us
    pallas_call x1, Pallas kernels: 39.2 us -> 38.6 us  [fused_body(): pl.pallas_call(functools.partial(layer_kernel, (kvn, tpn, kv_local, group...]
where the time goes in v3:
time: 39.4 us; the launch traced here: 39.2 us
  Pallas kernels  38.6 us (98%)
  local copies, waits for them, and re-layouts  0.6 us (2%)
    pallas_call x1, Pallas kernels, fused_body(): pl.pallas_call(functools.partial(layer_kernel, (kvn, tpn, kv_local, group...  38.6 us

profile of v3, /device:TPU:0, one launch (start us, length us, event | category | flops | bytes accessed | tf_op | source)
XLA Modules:
  0.0 39.2 jit_solution(4889639384285659515)
XLA Ops:
  0.0 38.6 %layer.1 = bf16[16,256]{1,0:T(8,128)(2,1)S(1)} custom-call(bf16[16,256]{1,0:T(8,128)(2,1)} %residual_ref.1, bf16[1024]{0:T(1024)(128)(2,1)} %norm_hbm.1, bf16[1024]{0:T(1024)(128)(2,1)} %mixer_hbm.1, bf16[128]{0:T(256)(128)(2,1)} %head_hbm.1, f32[4]{0:T(128)} %lambda_ref.1, bf16[16,2048,128]{2,1,0:T(8,128)(2,1)} %bitcast.2, bf16[16,2048,128]{2,1,0:T(8,128)(2,1)} %bitcast.3, ...), custom_call_target="tpu_custom_call" | custom-call | tf_op jit(solution)/shard_map/layer/pallas_call | solution.py:598
  38.6 0.6 %copy.15 = bf16[16,256]{1,0:T(8,128)(2,1)} copy(bf16[16,256]{1,0:T(8,128)(2,1)S(1)} %layer.1) | data formatting | bytes 16384
